TPU v7x, 32 devices: a whole 2x2x4 slice. The times are simulated.
32 devices in a mesh: kv: 4 (over y, x), tp: 8 (over z, core).
Axes of the slice: x: 2, y: 2, z: 4, core: 2. Of those that a mesh axis runs over, the one named last changes fastest.
Arguments:
- resid: bfloat16 [32, 4096], P('tp', 'kv'), may hold values from -35 to 35
- attn_gain: bfloat16 [4096], replicated, may hold values from 0.099609375 to 1.8984375
- w_query_nope: bfloat16 [4096, 8192], P('kv', 'tp'), may hold values from -0.09375 to 0.09375
- w_query_rope: bfloat16 [4096, 4096], P('kv', 'tp'), may hold values from -0.09375 to 0.09375
- w_latent: bfloat16 [4096, 512], P('kv'), may hold values from -0.09375 to 0.09375
- w_key_rope: bfloat16 [4096, 64], replicated, may hold values from -0.09375 to 0.09375
- latent_gain: bfloat16 [512], replicated, may hold values from 0.099609375 to 1.8984375
- key_up: bfloat16 [512, 64, 128], P(None, 'tp'), may hold values from -0.5 to 0.5
- value_up: bfloat16 [512, 64, 128], P(None, 'tp'), may hold values from -0.25 to 0.25
- w_out: bfloat16 [8192, 4096], P('tp', 'kv'), may hold values from -4 to 4
- post_gain: bfloat16 [4096], replicated, may hold values from 0.099609375 to 1.8984375
- mlp_gain: bfloat16 [4096], replicated, may hold values from 0.099609375 to 1.8984375
- w_gate: bfloat16 [4096, 11008], P('kv', 'tp'), may hold values from -3 to 3
- w_up: bfloat16 [4096, 11008], P('kv', 'tp'), may hold values from -3 to 3
- w_down: bfloat16 [11008, 4096], P('tp', 'kv'), may hold values from -0.0546875 to 0.0546875
- cache_latent: bfloat16 [32, 2048, 512], P('tp', 'kv'), may hold values from -6 to 6
- cache_rope_key: bfloat16 [32, 2048, 64], P('tp', 'kv'), may hold values from -740 to 740
Outputs:
- next_resid: bfloat16 [32, 4096], P('tp', 'kv')
- new_latent: bfloat16 [32, 512], P('tp')
- new_rope_key: bfloat16 [32, 64], P('tp')
All inputs are finite; a program needn't handle non-finite values.
Results may differ from a plain program's by a relative error of at most 0.035.
Values may be sent and summed in bfloat16 or wider, within the bound.
A program may use at most 64 MiB of HBM per device.

v0:
```python
import jax
import jax.numpy as jnp
from jax import lax
from jax.sharding import PartitionSpec as P

EPS = 1e-06
THETA = 10000.0


def rotate(vector, position):
    half_width = vector.shape[-1] // 2
    frequency = THETA ** (-jnp.arange(half_width, dtype=jnp.float32) / half_width)
    angles = jnp.asarray(position, jnp.float32) * frequency
    cos_table, sin_table = (jnp.cos(angles), jnp.sin(angles))
    lower_half, upper_half = (vector[..., :half_width], vector[..., half_width:])
    return jnp.concatenate(
        [
            lower_half * cos_table - upper_half * sin_table,
            lower_half * sin_table + upper_half * cos_table,
        ],
        axis=-1,
    )


def body(
    resid,
    attn_gain,
    w_query_nope,
    w_query_rope,
    w_latent,
    w_key_rope,
    latent_gain,
    key_up,
    value_up,
    w_out,
    post_gain,
    mlp_gain,
    w_gate,
    w_up,
    w_down,
    cache_latent,
    cache_rope_key,
):
    kv_count = lax.axis_size("kv")
    kv_index = lax.axis_index("kv")
    tp_index = lax.axis_index("tp")
    own_rows, width_dev = resid.shape
    model_width = width_dev * kv_count
    heads_dev = key_up.shape[1]
    pos_dev = cache_latent.shape[1]
    context = pos_dev * kv_count
    score_scale = (key_up.shape[2] + cache_rope_key.shape[2]) ** (-0.5)
    col_start = kv_index * width_dev
    row_start = tp_index * own_rows

    def block_of(vector):
        return lax.dynamic_slice_in_dim(vector, col_start, width_dev, 0).astype(jnp.float32)[
            None, :
        ]

    gathered = lax.all_gather(resid, "tp", axis=0, tiled=True)
    batch_rows = gathered.shape[0]
    gathered_float = gathered.astype(jnp.float32)
    normed_a = (gathered_float * block_of(attn_gain)).astype(jnp.bfloat16)
    own_normed = lax.dynamic_slice_in_dim(normed_a, row_start, own_rows, 0)
    key_rows = lax.dynamic_slice_in_dim(w_key_rope, col_start, width_dev, 0)
    q_nope_sum, q_rope_sum, latent_sum, key_sum, square_sum = (
        lax.psum(
            jnp.dot(normed_a, w_query_nope, preferred_element_type=jnp.float32).astype(
                jnp.bfloat16
            ),
            "kv",
        ).astype(jnp.float32),
        lax.psum(
            jnp.dot(normed_a, w_query_rope, preferred_element_type=jnp.float32).astype(
                jnp.bfloat16
            ),
            "kv",
        ).astype(jnp.float32),
        lax.psum(
            jnp.dot(own_normed, w_latent, preferred_element_type=jnp.float32).astype(jnp.bfloat16),
            "kv",
        ).astype(jnp.float32),
        lax.psum(
            jnp.dot(own_normed, key_rows, preferred_element_type=jnp.float32).astype(jnp.bfloat16),
            "kv",
        ).astype(jnp.float32),
        lax.psum(
            jnp.sum(gathered_float * gathered_float, axis=1).astype(jnp.bfloat16), "kv"
        ).astype(jnp.float32),
    )
    scale_in = lax.rsqrt(square_sum / model_width + EPS)[:, None]
    own_scale = lax.dynamic_slice_in_dim(scale_in, row_start, own_rows, 0)
    q_nope = (q_nope_sum * scale_in).astype(jnp.bfloat16).reshape(batch_rows, heads_dev, -1)
    q_rope = rotate((q_rope_sum * scale_in).reshape(batch_rows, heads_dev, -1), context).astype(
        jnp.bfloat16
    )
    new_latent = (
        latent_sum
        * lax.rsqrt(jnp.mean(latent_sum * latent_sum, axis=1, keepdims=True) + EPS)
        * latent_gain.astype(jnp.float32)[None, :]
    ).astype(jnp.bfloat16)
    new_rope_key = rotate(key_sum * own_scale, context).astype(jnp.bfloat16)
    q_lat = jnp.einsum("bhd,chd->bhc", q_nope, key_up, preferred_element_type=jnp.float32).astype(
        jnp.bfloat16
    )
    seq_lat, seq_rope = (
        lax.all_to_all(q_lat, "tp", split_axis=0, concat_axis=1, tiled=True),
        lax.all_to_all(q_rope, "tp", split_axis=0, concat_axis=1, tiled=True),
    )
    scores = (
        jnp.einsum("bhc,bpc->bhp", seq_lat, cache_latent, preferred_element_type=jnp.float32)
        + jnp.einsum("bhr,bpr->bhp", seq_rope, cache_rope_key, preferred_element_type=jnp.float32)
    ) * score_scale
    own_score = (
        jnp.einsum("bhc,bc->bh", seq_lat, new_latent, preferred_element_type=jnp.float32)
        + jnp.einsum("bhr,br->bh", seq_rope, new_rope_key, preferred_element_type=jnp.float32)
    ) * score_scale
    local_peak = jnp.maximum(jnp.max(scores, axis=2), own_score)
    peak = lax.pmax(local_peak, "kv")
    probs = jnp.exp(scores - peak[:, :, None])
    own_prob = jnp.exp(own_score - peak)
    totals = lax.psum(jnp.sum(probs, axis=2), "kv") + own_prob
    partial_value = jnp.einsum(
        "bhp,bpc->bhc", probs.astype(jnp.bfloat16), cache_latent, preferred_element_type=jnp.float32
    )
    summed = (
        lax.psum(partial_value.astype(jnp.bfloat16), "kv").astype(jnp.float32)
        + own_prob[:, :, None] * new_latent.astype(jnp.float32)[:, None, :]
    )
    o_lat = (summed / totals[:, :, None]).astype(jnp.bfloat16)
    head_lat = lax.all_to_all(o_lat, "tp", split_axis=1, concat_axis=0, tiled=True)
    o_heads = jnp.einsum(
        "bhc,che->bhe", head_lat, value_up, preferred_element_type=jnp.float32
    ).astype(jnp.bfloat16)
    o_flat = o_heads.reshape(batch_rows, -1)
    attended = lax.psum_scatter(
        jnp.dot(o_flat, w_out, preferred_element_type=jnp.float32).astype(jnp.bfloat16),
        "tp",
        scatter_dimension=0,
        tiled=True,
    ).astype(jnp.float32)
    post_square = lax.psum(jnp.sum(attended * attended, axis=1), "kv")
    post_part = attended * lax.rsqrt(post_square / model_width + EPS)[:, None] * block_of(post_gain)
    resid_mid = (resid.astype(jnp.float32) + post_part).astype(jnp.bfloat16)
    mid_rows = lax.all_gather(resid_mid, "tp", axis=0, tiled=True)
    mid_float = mid_rows.astype(jnp.float32)
    normed_m = (mid_float * block_of(mlp_gain)).astype(jnp.bfloat16)
    gate_part = jnp.dot(normed_m, w_gate, preferred_element_type=jnp.float32)
    up_part = jnp.dot(normed_m, w_up, preferred_element_type=jnp.float32)
    square_part = jnp.sum(mid_float * mid_float, axis=1)
    gate_sum, up_sum, mid_square = (
        lax.psum(gate_part.astype(jnp.bfloat16), "kv").astype(jnp.float32),
        lax.psum(up_part.astype(jnp.bfloat16), "kv").astype(jnp.float32),
        lax.psum(square_part.astype(jnp.bfloat16), "kv").astype(jnp.float32),
    )
    scale_mid = lax.rsqrt(mid_square / model_width + EPS)[:, None]
    hidden = (jax.nn.silu(gate_sum * scale_mid) * (up_sum * scale_mid)).astype(jnp.bfloat16)
    lowered = lax.psum_scatter(
        jnp.dot(hidden, w_down, preferred_element_type=jnp.float32).astype(jnp.bfloat16),
        "tp",
        scatter_dimension=0,
        tiled=True,
    ).astype(jnp.float32)
    next_resid = (resid_mid.astype(jnp.float32) + lowered).astype(jnp.bfloat16)
    return (next_resid, new_latent, new_rope_key)


def solution(mesh):
    return jax.shard_map(
        body,
        mesh=mesh,
        in_specs=(
            P("tp", "kv"),
            P(),
            P("kv", "tp"),
            P("kv", "tp"),
            P("kv", None),
            P(),
            P(),
            P(None, "tp", None),
            P(None, "tp", None),
            P("tp", "kv"),
            P(),
            P(),
            P("kv", "tp"),
            P("kv", "tp"),
            P("tp", "kv"),
            P("tp", "kv", None),
            P("tp", "kv", None),
        ),
        out_specs=(P("tp", "kv"), P("tp", None), P("tp", None)),
        check_vma=False,
    )
```

profile of v0, /device:TPU:0, one launch (start us, length us, event | category | flops | bytes accessed | tf_op | source)
XLA Modules:
  0.0 386.5 jit_solution(13030384441631528125)
XLA Ops:
  7.2 16.0 %all-gather = bf16[8,4,1024]{2,1,0:T(4,128)(2,1)S(1)} all-gather(bf16[1,4,1024]{2,1,0:T(4,128)(2,1)} %bitcast.69), channel_id=1, replica_groups=mesh['kv'=4,'tp'=8] {'tp'}, dimensions={0}, use_global_device_ids=true | all-gather | bytes 73728 | tf_op jit(solution)/shard_map/all_gather | solution.py:61
  24.1 1.0 convolution_convert_fusion.10
  25.2 1.5 convolution_convert_fusion.9
  26.6 1.5 convolution_convert_fusion.8
  28.1 16.7 %all-reduce.2 = (bf16[32]{0:T(256)(128)(2,1)S(1)}, bf16[32,512]{1,0:T(8,128)(2,1)S(1)}, bf16[4,512]{1,0:T(4,128)(2,1)S(1)}, bf16[4,64]{1,0:T(4,128)(2,1)S(1)}) all-reduce(bf16[32]{0:T(256)(128)(2,1)S(1)} %get-tuple-element.15, bf16[32,512]{1,0:T(8,128)(2,1)S(1)} %convolution_convert_fusion.8, ...), channel_id=1, replica_groups=mesh['kv'=4,'tp'=8] {'kv'}, use_global_device_ids=true, to_apply=%region_2.0 | all-reduce | flops 18720 | bytes 74880 | tf_op jit(solution)/shard_map/psum | solution.py:88
  46.0 4.6 %all-to-all-start.1 = ((bf16[8,2,1024]{2,1,0:T(2,128)(2,1)}), bf16[8,2,1024]{2,1,0:T(2,128)(2,1)S(1)}, u32[]{:S(2)}, u32[]{:S(2)}) async-start(bf16[8,2,1024]{2,1,0:T(2,128)(2,1)} %reshape.73), calls=%async_computation.1 | async-start | bytes 65536 | tf_op jit(solution)/shard_map/all_to_all | solution.py:109
  50.7 2.7 convolution_convert_fusion.7
  53.7 42.1 %all-reduce.10.cloned.1.call-done = bf16[32,1024]{1,0:T(8,128)(2,1)} async-done(((bf16[32,1024]{1,0:T(8,128)(2,1)}), bf16[32,1024]{1,0:T(8,128)(2,1)}) %all-reduce.10.cloned.1.call-update) | async-done | bytes 65552 | tf_op jit(solution)/shard_map/psum | solution.py:68
  95.8 1.8 fusion.1
  97.6 0.9 copy.35
  98.4 4.6 %all-to-all-start = ((bf16[32,8,512]{2,1,0:T(8,128)(2,1)}), bf16[32,8,512]{2,1,0:T(8,128)(2,1)S(1)}, u32[]{:S(2)}, u32[]{:S(2)}) async-start(bf16[32,8,512]{2,1,0:T(8,128)(2,1)} %copy.35), calls=%async_computation | async-start | bytes 524288 | tf_op jit(solution)/shard_map/all_to_all | solution.py:108
  103.5 9.3 %all-to-all-done = bf16[32,8,512]{2,1,0:T(8,128)(2,1)S(1)} async-done(((bf16[32,8,512]{2,1,0:T(8,128)(2,1)}), bf16[32,8,512]{2,1,0:T(8,128)(2,1)S(1)}, u32[]{:S(2)}, u32[]{:S(2)}) %all-to-all-start) | async-done | bytes 262176 | tf_op jit(solution)/shard_map/all_to_all | solution.py:108
  112.7 2.3 fusion.10
  115.3 1.3 fusion.48
  116.5 8.9 %pmax.7 = f32[4,64]{1,0:T(4,128)S(1)} all-reduce(f32[4,64]{1,0:T(4,128)S(1)} %fusion.39), channel_id=1, replica_groups=mesh['kv'=4,'tp'=8] {'kv'}, use_global_device_ids=true, to_apply=%region_8.0 | all-reduce | flops 256 | bytes 2048 | tf_op jit(solution)/shard_map/pmax | solution.py:120
  125.5 2.8 convolution_convert_fusion.2
  128.6 8.9 %psum.83 = f32[4,64]{1,0:T(4,128)S(1)} all-reduce(f32[4,64]{1,0:T(4,128)S(1)} %fusion.5), channel_id=1, replica_groups=mesh['kv'=4,'tp'=8] {'kv'}, use_global_device_ids=true, to_apply=%region_11.0 | all-reduce | flops 256 | bytes 2048 | tf_op jit(solution)/shard_map/psum | solution.py:123
  137.5 32.0 %all-reduce.12.cloned.1.call-done = bf16[4,64,512]{2,1,0:T(8,128)(2,1)} async-done(((bf16[4,64,512]{2,1,0:T(8,128)(2,1)}), bf16[4,64,512]{2,1,0:T(8,128)(2,1)}) %all-reduce.12.cloned.1.call-update) | async-done | bytes 262160 | tf_op jit(solution)/shard_map/psum | solution.py:128
  169.5 1.1 divide_convert_fusion
  170.9 14.1 %all_to_all.54 = bf16[4,64,512]{2,0,1:T(4,128)(2,1)S(1)} all-to-all(bf16[4,64,512]{2,0,1:T(4,128)(2,1)S(1)} %copy.38), channel_id=1, replica_groups=mesh['kv'=4,'tp'=8] {'tp'}, dimensions={1} | all-to-all | bytes 524288 | tf_op jit(solution)/shard_map/all_to_all | solution.py:132
  185.2 1.5 fusion.2
  186.7 2.7 convolution_convert_fusion.6
  191.4 50.8 %all-reduce.14.cloned.1.call-done = bf16[32,1024]{1,0:T(8,128)(2,1)} async-done(((bf16[32,1024]{1,0:T(8,128)(2,1)}), bf16[32,1024]{1,0:T(8,128)(2,1)}) %all-reduce.14.cloned.1.call-update) | async-done | bytes 65552
  243.8 9.8 %psum.84 = f32[4]{0:T(128)S(1)} all-reduce(f32[4]{0:T(128)S(1)} %fusion.28), channel_id=1, replica_groups=mesh['kv'=4,'tp'=8] {'kv'}, use_global_device_ids=true, to_apply=%region_14.0 | all-reduce | flops 4 | bytes 32 | tf_op jit(solution)/shard_map/psum | solution.py:143
  254.4 14.0 %all-gather.1 = bf16[8,4,1024]{2,1,0:T(4,128)(2,1)S(1)} all-gather(bf16[1,4,1024]{2,1,0:T(4,128)(2,1)S(1)} %bitcast.68), channel_id=1, replica_groups=mesh['kv'=4,'tp'=8] {'tp'}, dimensions={0}, use_global_device_ids=true | all-gather | bytes 73728 | tf_op jit(solution)/shard_map/all_gather | solution.py:146
  268.5 1.6 convolution_convert_fusion.1
  270.2 1.6 convolution_convert_fusion
  271.8 8.0 %psum.86 = bf16[32]{0:T(256)(128)(2,1)S(1)} all-reduce(bf16[32]{0:T(256)(128)(2,1)S(1)} %multiply_reduce_fusion), channel_id=1, replica_groups=mesh['kv'=4,'tp'=8] {'kv'}, use_global_device_ids=true, to_apply=%region_17.0 | all-reduce | flops 32 | bytes 128 | tf_op jit(solution)/shard_map/psum | solution.py:155
  279.8 40.7 %all-reduce.18.cloned.1.call-done = (bf16[32,1376]{1,0:T(8,128)(2,1)}, bf16[32,1376]{1,0:T(8,128)(2,1)}) async-done(((bf16[32,1376]{1,0:T(8,128)(2,1)}, bf16[32,1376]{1,0:T(8,128)(2,1)}), (bf16[32,1376]{1,0:T(8,128)(2,1)}, bf16[32,1376]{1,0:T(8,128)(2,1)})) %all-reduce.18.cloned.1.call-update) | async-done | bytes 176144 | tf_op jit(solution)/shard_map/psum | solution.py:154
  320.5 3.2 convolution_convert_fusion.5
  324.4 54.3 %all-reduce.16.cloned.1.call-done = bf16[32,1024]{1,0:T(8,128)(2,1)} async-done(((bf16[32,1024]{1,0:T(8,128)(2,1)}), bf16[32,1024]{1,0:T(8,128)(2,1)}) %all-reduce.16.cloned.1.call-update) | async-done | bytes 65552
  378.6 1.3 add_convert_fusion.1
  (60 shorter events, 8.2 us)
Async XLA Ops:
  7.2 261.3 %copy-start = (bf16[1024,1376]{0,1:T(8,128)(2,1)S(1)}, bf16[1024,1376]{0,1:T(8,128)(2,1)}, u32[]{:S(2)}) copy-start(bf16[1024,1376]{0,1:T(8,128)(2,1)} %param.29) | copy-start | bytes 8454148
  46.0 52.5 %all-to-all-start.1 = ((bf16[8,2,1024]{2,1,0:T(2,128)(2,1)}), bf16[8,2,1024]{2,1,0:T(2,128)(2,1)S(1)}, u32[]{:S(2)}, u32[]{:S(2)}) async-start(bf16[8,2,1024]{2,1,0:T(2,128)(2,1)} %reshape.73), calls=%async_computation.1 | async-start | bytes 65536 | tf_op jit(solution)/shard_map/all_to_all | solution.py:109
  50.6 52.6 %copy-start.4 = (bf16[512]{0:T(512)(128)(2,1)S(1)}, bf16[512]{0:T(512)(128)(2,1)}, u32[]{:S(2)}) copy-start(bf16[512]{0:T(512)(128)(2,1)} %param.23) | copy-start | bytes 3076
  50.6 45.2 %all-reduce.10.cloned.1.call-start = ((), (), s32[]{:S(2)}) async-start(), calls=%async_computation.3 | async-start | bytes 131072 | tf_op jit(solution)/shard_map/psum | solution.py:68
  98.4 14.3 %all-to-all-start = ((bf16[32,8,512]{2,1,0:T(8,128)(2,1)}), bf16[32,8,512]{2,1,0:T(8,128)(2,1)S(1)}, u32[]{:S(2)}, u32[]{:S(2)}) async-start(bf16[32,8,512]{2,1,0:T(8,128)(2,1)} %copy.35), calls=%async_computation | async-start | bytes 524288 | tf_op jit(solution)/shard_map/all_to_all | solution.py:108
  103.0 66.5 %all-reduce.12.cloned.1.call-start = ((), (), s32[]{:S(2)}) async-start(), calls=%async_computation.4 | async-start | bytes 524288 | tf_op jit(solution)/shard_map/psum | solution.py:128
  103.2 13.3 %copy-start.3 = (bf16[4,512]{1,0:T(4,128)(2,1)}, bf16[4,512]{1,0:T(4,128)(2,1)S(1)}, u32[]{:S(2)}) copy-start(bf16[4,512]{1,0:T(4,128)(2,1)S(1)} %get-tuple-element.10) | copy-start | bytes 12292
  128.3 113.9 %all-reduce.14.cloned.1.call-start = ((), (), s32[]{:S(2)}) async-start(), calls=%async_computation.5 | async-start | bytes 131072
  185.1 5.1 %copy-start.5 = (u32[32]{0:T(128)S(1)}, u32[32]{0:T(128)}, u32[]{:S(2)}) copy-start(u32[32]{0:T(128)} %constant.53) | copy-start | bytes 388
  185.1 68.5 %copy-start.2 = (bf16[4,1024]{1,0:T(4,128)(2,1)S(1)}, bf16[4,1024]{1,0:T(4,128)(2,1)}, u32[]{:S(2)}) copy-start(bf16[4,1024]{1,0:T(4,128)(2,1)} %param.17) | copy-start | bytes 24580
  189.4 131.1 %all-reduce.18.cloned.1.call-start = ((), (), s32[]{:S(2)}) async-start(), calls=%async_computation.7 | async-start | bytes 360448 | tf_op jit(solution)/shard_map/psum | solution.py:154
  268.4 1.8 copy-start.1
  279.7 98.9 %all-reduce.16.cloned.1.call-start = ((), (), s32[]{:S(2)}) async-start(), calls=%async_computation.6 | async-start | bytes 131072
Sparse Core Ops, SparseCore 0:
  54.3 41.4 all-reduce.9
  128.4 41.0 all-reduce.11
  189.5 52.6 all-reduce.13
  279.9 40.6 all-reduce.17
  323.9 54.7 all-reduce.15
where the time goes:
time: 388 us; the launch traced here: 386 us
  waiting for transfers between devices  229 us (59%)
  blocking collectives  96.5 us (25%)
  matrix products  25.8 us (7%)
  between operations  14.6 us (4%)
  starting transfers between devices  9.46 us (2%)
  other arithmetic  8.04 us (2%)
    unnamed x7, waiting for transfers between devices  105 us
    psum x1, waiting for transfers between devices, body(): lax.psum(jnp.dot(normed_a, w_query_nope, preferred_element_type=jnp.float...  42.1 us
    psum x1, waiting for transfers between devices, body(): lax.psum(up_part.astype(jnp.bfloat16), 'kv').astype(jnp.float32)  40.7 us
    psum x1, waiting for transfers between devices, body(): lax.psum(partial_value.astype(jnp.bfloat16), 'kv').astype(jnp.float32)  32 us
    psum x1, blocking collectives, body(): lax.psum(jnp.sum(gathered_float * gathered_float, axis=1).astype(jnp.bflo...  16.7 us
    all_gather x1, blocking collectives, body(): gathered = lax.all_gather(resid, 'tp', axis=0, tiled=True)  16 us
    all_to_all x1, blocking collectives, body(): lax.all_to_all(o_lat, 'tp', split_axis=1, concat_axis=0, tiled=True)  14.1 us
    all_gather x1, blocking collectives, body(): mid_rows = lax.all_gather(resid_mid, 'tp', axis=0, tiled=True)  14 us
  transfers between devices with their start and end apart: 7, of which 6 were waited for; matrix products, arithmetic and copies ran while one was open for 2% of the time, Pallas kernels for 0%

commit v1 on v0

--- a/solution.py
+++ b/solution.py
@@ -1,6 +1,11 @@
+import functools
+
 import jax
 import jax.numpy as jnp
+import numpy as np
 from jax import lax
+from jax.experimental import pallas as pl
+from jax.experimental.pallas import tpu as pltpu
 from jax.sharding import PartitionSpec as P
 
 EPS = 1e-06
@@ -166,9 +171,383 @@
     return (next_resid, new_latent, new_rope_key)
 
 
+F32 = jnp.float32
+BF16 = jnp.bfloat16
+MESH = pl.DeviceIdType.MESH
+
+
+def dot_nt(a, b):
+    return lax.dot_general(a, b, (((1,), (1,)), ((), ())), preferred_element_type=F32)
+
+
+def lane_iota(shape):
+    return lax.broadcasted_iota(jnp.int32, shape, len(shape) - 1)
+
+
+def turn(v, cos, sin, half):
+    width = v.shape[-1]
+    low = lane_iota(v.shape) % (2 * half) < half
+    swapped = jnp.where(low, pltpu.roll(v, width - half, 1), pltpu.roll(v, half, 1))
+    return v * cos + swapped * sin
+
+
+def layer_kernel(
+    K, T, position_count,
+    resid, attn_gain, latent_gain, post_gain, mlp_gain, cos_ref, sin_ref,
+    h_wqn, h_wqr, h_wlat, h_wkr, h_ku, h_vu, h_wo, h_wg, h_wu, h_wd, h_cl, h_cr,
+    out, out_lat, out_key,
+    wqn, wqr, wlat, wkr, ku, vu, wo, wg, wu, wd, cl, cr,
+    xbuf, xf, qs, qrv, sqs, sqr, lats, latr, qe, qbuf, accs, accr, mls, mlr,
+    nls, nks, osend, obuf, ohs, h3, tall, es, er, ab, sqas, sqa, psq, attf, mids,
+    gs, us, gr, ur, sqms, sqmr, hb, ls, lr,
+    wsem, ssem, rsem,
+):
+    k = lax.axis_index("kv")
+    t = lax.axis_index("tp")
+    R, W = resid.shape
+    D = W * K
+    B = R * T
+    LAT = h_wlat.shape[1]
+    ROPE = h_wkr.shape[1]
+    QN = h_wqn.shape[1]
+    QR = h_wqr.shape[1]
+    HD = QR // ROPE
+    NOPE = QN // HD
+    H = HD * T
+    VD = h_vu.shape[1] // HD
+    half = ROPE // 2
+    score_scale = (NOPE + ROPE) ** (-0.5)
+    col = pl.ds(pl.multiple_of(k * W, 128), W)
+
+    loads = {}
+    pairs = [
+        ("qn", h_wqn, wqn), ("qr", h_wqr, wqr), ("lat", h_wlat, wlat),
+        ("kr", h_wkr.at[col], wkr), ("ku", h_ku, ku), ("cl", h_cl, cl), ("cr", h_cr, cr),
+        ("vu", h_vu, vu), ("wo", h_wo, wo), ("wg", h_wg, wg), ("wu", h_wu, wu), ("wd", h_wd, wd),
+    ]
+    for i, (name, src, dst) in enumerate(pairs):
+        loads[name] = pltpu.make_async_copy(src, dst, wsem.at[i])
+        loads[name].start()
+
+    others = [(a, b) for a in range(K) for b in range(T) if (a, b) != (0, 0)]
+    tps = [(0, b) for b in range(1, T)]
+    kvs = [(a, 0) for a in range(1, K)]
+
+    def peer(off):
+        return lax.rem(k + off[0], K), lax.rem(t + off[1], T)
+
+    barrier = pltpu.get_barrier_semaphore()
+    for off in others:
+        pl.semaphore_signal(barrier, inc=1, device_id=peer(off), device_id_type=MESH)
+
+    sent = []
+
+    def send(src, dst, off):
+        i = len(sent)
+        copy = pltpu.make_async_remote_copy(
+            src_ref=src, dst_ref=dst, send_sem=ssem.at[i], recv_sem=rsem.at[i],
+            device_id=peer(off), device_id_type=MESH,
+        )
+        copy.start()
+        sent.append(copy)
+        return copy
+
+    def arrive(copies):
+        for copy in copies:
+            copy.wait_recv()
+
+    def dot(a, b):
+        return jnp.dot(a, b[...], preferred_element_type=F32)
+
+    def put_rows(ref, s, v):
+        for c in range(ref.shape[0]):
+            ref[c, pl.ds(s, R, stride=T), :] = v[:, c * 128:(c + 1) * 128]
+
+    def rows(ref, s):
+        return jnp.concatenate(
+            [ref[c, pl.ds(s, R, stride=T), :] for c in range(ref.shape[0])], axis=1
+        )
+
+    def put_all(ref, v):
+        for c in range(ref.shape[0]):
+            ref[c] = v[:, c * 128:(c + 1) * 128]
+
+    def all_rows(ref):
+        return jnp.concatenate([ref[c] for c in range(ref.shape[0])], axis=1)
+
+    pl.semaphore_wait(barrier, len(others))
+
+    copies = [send(resid, xbuf.at[t], off) for off in tps]
+    xo = resid[...].astype(F32)
+    xbuf[pl.ds(t, 1)] = resid[...][None]
+    again = attn_gain[:, col].astype(F32)
+    own_normed = (xo * again).astype(BF16)
+    loads["lat"].wait()
+    loads["kr"].wait()
+    lats[:, :LAT] = dot(own_normed, wlat)
+    lats[:, LAT:LAT + ROPE] = dot(own_normed, wkr)
+    lats[:, LAT + ROPE:] = jnp.broadcast_to(
+        jnp.sum(xo * xo, axis=1, keepdims=True), (R, lats.shape[1] - LAT - ROPE)
+    )
+    latr[pl.ds(k, 1)] = lats[...][None]
+    lat_copies = [send(lats, latr.at[k], off) for off in kvs]
+    arrive(copies)
+    for s in range(T):
+        put_rows(xf, s, xbuf[s].astype(F32))
+    x = all_rows(xf)
+    normed = (x * again).astype(BF16)
+    sqs[...] = jnp.broadcast_to(jnp.sum(x * x, axis=1, keepdims=True), (B, 128)).reshape(K, T, 128)
+    loads["qn"].wait()
+    qs[:, :, :QN] = dot(normed, wqn).reshape(K, T, QN).astype(BF16)
+    loads["qr"].wait()
+    qs[:, :, QN:] = dot(normed, wqr).reshape(K, T, QR).astype(BF16)
+    copies = []
+    for off in kvs:
+        to = peer(off)[0]
+        copies.append(send(qs.at[to], qrv.at[k], off))
+        copies.append(send(sqs.at[to], sqr.at[k], off))
+    qrv[pl.ds(k, 1)] = qs[pl.ds(k, 1)]
+    sqr[pl.ds(k, 1)] = sqs[pl.ds(k, 1)]
+
+    arrive(lat_copies)
+    lat = sum(latr[s] for s in range(K))
+    raw = lat[:, :LAT]
+    new_lat = (
+        raw * lax.rsqrt(jnp.mean(raw * raw, axis=1, keepdims=True) + EPS)
+        * latent_gain[...].astype(F32)
+    ).astype(BF16)
+    own_scale = lax.rsqrt(lat[:, LAT + ROPE:LAT + ROPE + 1] / D + EPS)
+    tail = lat[:, LAT:]
+    turned = turn(tail * own_scale, cos_ref[:, :tail.shape[1]], sin_ref[:, :tail.shape[1]], half)
+    new_key = jnp.where(lane_iota(turned.shape) < ROPE, turned, 0.0).astype(BF16)
+    out_lat[...] = new_lat
+    out_key[...] = new_key[:, :ROPE]
+    nls[...] = new_lat.astype(F32)
+    nks[...] = new_key.astype(F32)
+
+    arrive(copies)
+    q = sum(qrv[s].astype(F32) for s in range(K))
+    scale = lax.rsqrt(sum(sqr[s] for s in range(K))[:, :1] / D + EPS)
+    q_nope = (q[:, :QN] * scale).astype(BF16).astype(F32)
+    q_rope = turn(q[:, QN:] * scale, cos_ref[...], sin_ref[...], half).astype(BF16).astype(F32)
+
+    def own_head(width, each):
+        shape = (HD, width)
+        return lane_iota(shape) // each == lax.broadcasted_iota(jnp.int32, shape, 0)
+
+    def spread(v, each):
+        mask = own_head(v.shape[1], each)
+        return jnp.concatenate(
+            [jnp.where(mask, jnp.broadcast_to(v[i:i + 1], mask.shape), 0.0) for i in range(T)], axis=0
+        ).astype(BF16)
+
+    RP = qe.shape[2] - LAT
+    fold_shape = (QR, RP)
+    fold = (
+        lax.broadcasted_iota(jnp.int32, fold_shape, 0) % ROPE == lane_iota(fold_shape)
+    ).astype(F32).astype(BF16)
+    qe[:, :, LAT:] = jnp.dot(
+        spread(q_rope, ROPE), fold, preferred_element_type=F32
+    ).reshape(T, HD, RP).astype(BF16)
+    loads["ku"].wait()
+    qe[:, :, :LAT] = dot_nt(spread(q_nope, NOPE), ku[...]).reshape(T, HD, LAT).astype(BF16)
+    copies = [send(qe.at[peer(off)[1]], qbuf.at[k, t], off) for off in others]
+    qbuf[pl.ds(k, 1), pl.ds(t, 1)] = qe[pl.ds(t, 1)][None]
+    loads["cl"].wait()
+    loads["cr"].wait()
+    arrive(copies)
+
+    copies = []
+    for off in kvs + [(0, 0)]:
+        b = peer(off)[0]
+        qb32 = qbuf[pl.ds(b, 1)][0].astype(F32).reshape(H, LAT + RP)
+        qb = qb32.astype(BF16)
+        keys = cl[pl.ds(b, 1)][0]
+        scores = (
+            dot_nt(qb[:, :LAT], keys) + dot_nt(qb[:, LAT:LAT + ROPE], cr[pl.ds(b, 1)][0])
+        ) * score_scale
+        m = jnp.max(scores, axis=1, keepdims=True)
+        p = jnp.exp(scores - m)
+        total = jnp.sum(p, axis=1, keepdims=True)
+        acc = jnp.dot(p.astype(BF16), keys, preferred_element_type=F32).astype(BF16)
+        ml = jnp.where(lane_iota((H, 128)) < 64, m, total)
+        if off == (0, 0):
+            accr[pl.ds(k, 1)] = acc[None]
+            mlr[pl.ds(k, 1)] = ml[None]
+        else:
+            mls[off[0]] = ml
+            accs[off[0]] = acc
+            copies.append(send(mls.at[off[0]], mlr.at[k], off))
+            copies.append(send(accs.at[off[0]], accr.at[k], off))
+    nl = nls[pl.ds(k, 1), :]
+    nk = nks[pl.ds(k, 1), :]
+    own_score = (
+        jnp.sum(qb32[:, :LAT] * nl, axis=1, keepdims=True)
+        + jnp.sum(qb32[:, LAT:] * nk, axis=1, keepdims=True)
+    ) * score_scale
+    arrive(copies)
+    peaks = [mlr[s][:, :1] for s in range(K)]
+    peak = own_score
+    for m in peaks:
+        peak = jnp.maximum(peak, m)
+    own_prob = jnp.exp(own_score - peak)
+    total = own_prob
+    summed = own_prob * nl
+    for s in range(K):
+        w = jnp.exp(peaks[s] - peak)
+        total = total + w * mlr[s][:, 64:65]
+        summed = summed + w * accr[s].astype(F32)
+    osend[...] = (summed / total).reshape(T, HD, LAT).astype(BF16)
+    copies = [send(osend.at[peer(off)[1]], obuf.at[t], off) for off in tps]
+    obuf[pl.ds(t, 1)] = osend[pl.ds(t, 1)]
+    loads["vu"].wait()
+    arrive(copies)
+    wide = dot(obuf[...].astype(F32).reshape(T * HD, LAT).astype(BF16), vu)
+    mask = own_head(HD * VD, VD)
+    for i in range(T):
+        ohs[i:i + 1, :] = jnp.sum(
+            jnp.where(mask, wide[i * HD:(i + 1) * HD], 0.0), axis=0, keepdims=True
+        )
+    h3[pl.ds(k, 1)] = ohs[...].astype(BF16)[None]
+    copies = [send(h3.at[k], h3.at[k], off) for off in kvs]
+    loads["wo"].wait()
+    arrive(copies)
+    put_all(tall, dot(h3[...].astype(F32).reshape(B, HD * VD).astype(BF16), wo))
+    for s in range(T):
+        es[s] = rows(tall, s).astype(BF16)
+    copies = [send(es.at[peer(off)[1]], er.at[t], off) for off in tps]
+    er[pl.ds(t, 1)] = es[pl.ds(t, 1)]
+    arrive(copies)
+    attended = sum(er[s].astype(F32) for s in range(T))
+    sqas[...] = jnp.broadcast_to(jnp.sum(attended * attended, axis=1, keepdims=True), (R, 128))
+    ab[pl.ds(t, 1)] = attended.astype(BF16)[None]
+    copies = [send(sqas, sqa.at[k, t], off) for off in others]
+    copies += [send(ab.at[t], ab.at[t], off) for off in tps]
+    sqa[pl.ds(k, 1), pl.ds(t, 1)] = sqas[...][None, None]
+    arrive(copies)
+    for s in range(T):
+        put_rows(attf, s, ab[s].astype(F32))
+        psq[pl.ds(s, R, stride=T), :] = sum(sqa[j, s] for j in range(K))
+    post_scale = lax.rsqrt(psq[...][:, :1] / D + EPS)
+    mid = (
+        x + all_rows(attf) * post_scale * post_gain[:, col].astype(F32)
+    ).astype(BF16).astype(F32)
+    put_all(mids, mid)
+    normed_m = (mid * mlp_gain[:, col].astype(F32)).astype(BF16)
+    sqms[...] = jnp.broadcast_to(
+        jnp.sum(mid * mid, axis=1, keepdims=True), (B, 128)
+    ).reshape(K, T, 128)
+    FD = wg.shape[1]
+    loads["wg"].wait()
+    gs[...] = dot(normed_m, wg).reshape(K, T, FD).astype(BF16)
+    copies = [send(gs.at[peer(off)[0]], gr.at[k], off) for off in kvs]
+    copies += [send(sqms.at[peer(off)[0]], sqmr.at[k], off) for off in kvs]
+    loads["wu"].wait()
+    us[...] = dot(normed_m, wu).reshape(K, T, FD).astype(BF16)
+    copies += [send(us.at[peer(off)[0]], ur.at[k], off) for off in kvs]
+    gr[pl.ds(k, 1)] = gs[pl.ds(k, 1)]
+    ur[pl.ds(k, 1)] = us[pl.ds(k, 1)]
+    sqmr[pl.ds(k, 1)] = sqms[pl.ds(k, 1)]
+    arrive(copies)
+    mid_scale = lax.rsqrt(sum(sqmr[s] for s in range(K))[:, :1] / D + EPS)
+    gate = sum(gr[s].astype(F32) for s in range(K)) * mid_scale
+    up = sum(ur[s].astype(F32) for s in range(K)) * mid_scale
+    hb[pl.ds(k, 1)] = (gate / (1.0 + jnp.exp(-gate)) * up).astype(BF16)[None]
+    copies = [send(hb.at[k], hb.at[k], off) for off in kvs]
+    loads["wd"].wait()
+    arrive(copies)
+    put_all(tall, dot(hb[...].astype(F32).reshape(B, FD).astype(BF16), wd))
+    for s in range(T):
+        ls[s] = rows(tall, s).astype(BF16)
+    copies = [send(ls.at[peer(off)[1]], lr.at[t], off) for off in tps]
+    lr[pl.ds(t, 1)] = ls[pl.ds(t, 1)]
+    mid_own = rows(mids, t)
+    arrive(copies)
+    lowered = sum(lr[s].astype(F32) for s in range(T))
+    out[...] = (mid_own + lowered).astype(BF16)
+    for copy in sent:
+        copy.wait_send()
+
+
+def fused(
+    resid, attn_gain, w_query_nope, w_query_rope, w_latent, w_key_rope, latent_gain, key_up,
+    value_up, w_out, post_gain, mlp_gain, w_gate, w_up, w_down, cache_latent, cache_rope_key,
+):
+    K = lax.axis_size("kv")
+    T = lax.axis_size("tp")
+    R, W = resid.shape
+    LAT, HD, _ = key_up.shape
+    key_flat = key_up.reshape(LAT, -1)
+    value_flat = value_up.reshape(LAT, -1)
+    ROPE = w_key_rope.shape[1]
+    half = ROPE // 2
+    context = cache_latent.shape[1] * K
+    angle = context * THETA ** (-np.arange(half, dtype=np.float64) / half)
+    cos = np.tile(np.cos(angle), 2 * HD)[None].astype(np.float32)
+    sin = np.tile(np.concatenate([-np.sin(angle), np.sin(angle)]), HD)[None].astype(np.float32)
+    B = R * T
+    H = HD * T
+    QN, QR, FD, HV = w_query_nope.shape[1], w_query_rope.shape[1], w_gate.shape[1], value_flat.shape[1]
+    big = (w_query_nope, w_query_rope, w_latent, w_key_rope, key_flat, value_flat, w_out, w_gate,
+           w_up, w_down, cache_latent, cache_rope_key)
+
+    def held(a):
+        return pltpu.VMEM((W, ROPE) if a is w_key_rope else a.shape, a.dtype)
+
+    def bf(*shape):
+        return pltpu.VMEM(shape, BF16)
+
+    def fl(*shape):
+        return pltpu.VMEM(shape, F32)
+
+    LW = LAT + 128
+    slabs = fl(W // 128, B, 128)
+    scratch = [held(a) for a in big] + [
+        bf(T, R, W), slabs, bf(K, T, QN + QR), bf(K, T, QN + QR), fl(K, T, 128), fl(K, T, 128),
+        fl(R, LW), fl(K, R, LW), bf(T, HD, LW), bf(K, T, HD, LW), bf(K, H, LAT), bf(K, H, LAT),
+        fl(K, H, 128), fl(K, H, 128), fl(R, LAT), fl(R, 128), bf(T, HD, LAT), bf(T, HD, LAT),
+        fl(T, HV), bf(K, T, HV), slabs, bf(T, R, W), bf(T, R, W), bf(T, R, W),
+        fl(R, 128), fl(K, T, R, 128), fl(B, 128), slabs, slabs,
+        bf(K, T, FD), bf(K, T, FD), bf(K, T, FD), bf(K, T, FD), fl(K, T, 128), fl(K, T, 128),
+        bf(K, T, FD), bf(T, R, W), bf(T, R, W),
+    ]
+    count = 10 * (K - 1) + 5 * (T - 1) + 2 * (K * T - 1) + 8
+    vmem = pl.BlockSpec(memory_space=pltpu.VMEM)
+    hbm = pl.BlockSpec(memory_space=pl.ANY)
+    return pl.pallas_call(
+        functools.partial(layer_kernel, K, T, context),
+        out_shape=(
+            jax.ShapeDtypeStruct((R, W), BF16),
+            jax.ShapeDtypeStruct((R, LAT), BF16),
+            jax.ShapeDtypeStruct((R, ROPE), BF16),
+        ),
+        in_specs=[vmem] * 7 + [hbm] * len(big),
+        out_specs=(vmem, vmem, vmem),
+        scratch_shapes=scratch + [
+            pltpu.SemaphoreType.DMA((len(big),)),
+            pltpu.SemaphoreType.DMA((count,)),
+            pltpu.SemaphoreType.DMA((count,)),
+        ],
+        compiler_params=pltpu.CompilerParams(
+            collective_id=0, has_side_effects=True, vmem_limit_bytes=60 * 1024 * 1024
+        ),
+    )(
+        resid, attn_gain[None], latent_gain[None], post_gain[None], mlp_gain[None],
+        jnp.asarray(cos), jnp.asarray(sin), *big,
+    )
+
+
+def layer(*args):
+    resid, key_up = args[0], args[7]
+    kv, tp = lax.axis_size("kv"), lax.axis_size("tp")
+    if resid.shape[0] == kv and key_up.shape[1] == 8 and tp == 8 and resid.shape[1] % 128 == 0:
+        return fused(*args)
+    return body(*args)
+
+
 def solution(mesh):
     return jax.shard_map(
-        body,
+        layer,
         mesh=mesh,
         in_specs=(
             P("tp", "kv"),

time: 388 us -> 91.2 us (0.24)
  waiting for transfers between devices: 229 us -> 0 us
  blocking collectives: 96.5 us -> 0 us
  Pallas kernels: 0 us -> 65.6 us
  matrix products: 25.8 us -> 0 us
  local copies, waits for them, and re-layouts: 2.91 us -> 24.4 us
  between operations: 14.6 us -> 0.64 us
  starting transfers between devices: 9.46 us -> 0 us
  other arithmetic: 8.04 us -> 0 us
    psum x3 -> x0, waiting for transfers between devices: 115 us -> none  [the longest x1 42.1 us: body(): lax.psum(jnp.dot(normed_a, w_query_nope, preferred_element_type=jnp.float...]
    unnamed x7 -> x0, waiting for transfers between devices: 105 us -> none
    pallas_call x0 -> x1, Pallas kernels: none -> 65.6 us  [fused(): pl.pallas_call(functools.partial(layer_kernel, K, T, context), out_shape=...]
    psum x4 -> x0, blocking collectives: 43.4 us -> none  [the longest x1 16.7 us: body(): lax.psum(jnp.sum(gathered_float * gathered_float, axis=1).astype(jnp.bflo...]
    all_gather x2 -> x0, blocking collectives: 30 us -> none  [the longest x1 16 us: body(): gathered = lax.all_gather(resid, 'tp', axis=0, tiled=True)]
    dot_general x15 -> x0, matrix products: 25.8 us -> none  [the longest x1 3.18 us: body(): jnp.dot(hidden, w_down, preferred_element_type=jnp.float32)]
    unnamed x15 -> x9, local copies, waits for them, and re-layouts: 1.5 us -> 15.8 us
    all_to_all x1 -> x0, blocking collectives: 14.1 us -> none  [body(): lax.all_to_all(o_lat, 'tp', split_axis=1, concat_axis=0, tiled=True)]
  transfers between devices with their start and end apart: 7 -> 0, of which waited for: 6 -> 0; matrix products, arithmetic and copies ran while one was open for 2% -> 0% of each run, Pallas kernels for 0% -> 0%
where the time goes in v1:
time: 91.2 us; the launch traced here: 90.6 us
  Pallas kernels  65.6 us (72%)
  local copies, waits for them, and re-layouts  24.4 us (27%)
    pallas_call x1, Pallas kernels, fused(): pl.pallas_call(functools.partial(layer_kernel, K, T, context), out_shape=...  65.6 us
    unnamed x9, local copies, waits for them, and re-layouts  15.8 us
    reshape x1, local copies, waits for them, and re-layouts, fused(): value_flat = value_up.reshape(LAT, -1)  3.46 us

profile of v1, /device:TPU:0, one launch (start us, length us, event | category | flops | bytes accessed | tf_op | source)
XLA Modules:
  0.0 90.6 jit_solution(3177354835493879951)
XLA Ops:
  0.6 1.3 %broadcast_in_dim.13.latent_gain = bf16[1,512]{1,0:T(2,128)(2,1)} reshape(bf16[512]{0:T(512)(128)(2,1)} %param.25) | data formatting | bytes 2048 | tf_op jit(solution)/shard_map/broadcast_in_dim | solution.py:535
  1.9 1.3 %broadcast_in_dim.12.attn_gain = bf16[1,4096]{1,0:T(2,128)(2,1)} reshape(bf16[4096]{0:T(1024)(128)(2,1)} %param.20) | data formatting | bytes 16384 | tf_op jit(solution)/shard_map/broadcast_in_dim | solution.py:535
  3.2 1.3 %broadcast_in_dim.14.post_gain = bf16[1,4096]{1,0:T(2,128)(2,1)} reshape(bf16[4096]{0:T(1024)(128)(2,1)} %param.29) | data formatting | bytes 16384 | tf_op jit(solution)/shard_map/broadcast_in_dim | solution.py:535
  4.5 1.3 %broadcast_in_dim.15.mlp_gain = bf16[1,4096]{1,0:T(2,128)(2,1)} reshape(bf16[4096]{0:T(1024)(128)(2,1)} %param.30) | data formatting | bytes 16384 | tf_op jit(solution)/shard_map/broadcast_in_dim | solution.py:535
  5.8 2.0 %copy.25.h_cr = bf16[4,512,64]{2,1,0:T(8,128)(2,1)} copy(bf16[4,512,64]{1,2,0:T(8,128)(2,1)} %param.35) | data formatting | bytes 524288 | tf_op args[16]
  7.8 0.0 copy-start
  7.8 2.5 %copy.22.h_wkr = bf16[4096,64]{1,0:T(8,128)(2,1)} copy(bf16[4096,64]{0,1:T(8,128)(2,1)} %param.24) | data formatting | bytes 1048576 | tf_op args[5]
  10.3 3.5 %copy_bitcast_fusion = (bf16[512,1024]{1,0:T(8,128)(2,1)}, bf16[512,1024]{1,0:T(8,128)(2,1)}) fusion(bf16[64,8,8,128]{3,2,1,0:T(8,128)(2,1)} %bitcast.6, bf16[64,8,8,128]{3,2,1,0:T(8,128)(2,1)} %bitcast.7), kind=kLoop, calls=%fused_computation | loop fusion | bytes 4194304 | tf_op jit(solution)/shard_map/reshape | solution.py:481
  13.8 0.0 copy-done
  13.8 2.9 %copy.23.h_wg = bf16[1024,1376]{1,0:T(8,128)(2,1)} copy(bf16[1024,1376]{0,1:T(8,128)(2,1)S(1)} %copy-done) | data formatting | bytes 5636096 | tf_op args[12]
  16.7 4.5 %copy.24.h_wu = bf16[1024,1376]{1,0:T(8,128)(2,1)} copy(bf16[1024,1376]{0,1:T(8,128)(2,1)} %param.32) | data formatting | bytes 5636096 | tf_op args[13]
  21.2 65.6 %shard_map.202 = (bf16[4,1024]{1,0:T(4,128)(2,1)}, bf16[4,512]{1,0:T(4,128)(2,1)}, bf16[4,64]{1,0:T(4,128)(2,1)}) custom-call(bf16[4,1024]{1,0:T(4,128)(2,1)} %resid.1, bf16[1,4096]{1,0:T(2,128)(2,1)} %broadcast_in_dim.12.attn_gain, bf16[1,512]{1,0:T(2,128)(2,1)} %broadcast_in_dim.13.latent_gain, bf16[1,4096]{1,0:T(2,128)(2,1)} %broadcast_in_dim.14.post_gain, ...), custom_call_target="tpu_custom_call" | custom-call | tf_op jit(solution)/shard_map/pallas_call | solution.py:517
  86.8 1.3 %copy.33 = bf16[4,1024]{1,0:T(4,128)(2,1)} copy(bf16[4,1024]{1,0:T(4,128)(2,1)} %get-tuple-element.8) | data formatting | bytes 16384
  88.1 1.3 %copy.34 = bf16[4,512]{1,0:T(4,128)(2,1)} copy(bf16[4,512]{1,0:T(4,128)(2,1)} %get-tuple-element.9) | data formatting | bytes 8192
  89.4 1.2 %copy.35 = bf16[4,64]{1,0:T(4,128)(2,1)} copy(bf16[4,64]{1,0:T(4,128)(2,1)} %get-tuple-element.10) | data formatting | bytes 1024
Async XLA Ops:
  7.8 6.0 %copy-start = (bf16[1024,1376]{0,1:T(8,128)(2,1)S(1)}, bf16[1024,1376]{0,1:T(8,128)(2,1)}, u32[]{:S(2)}) copy-start(bf16[1024,1376]{0,1:T(8,128)(2,1)} %param.31) | copy-start | bytes 8454148

commit v2 on v1

--- a/solution.py
+++ b/solution.py
@@ -199,7 +199,7 @@
     wqn, wqr, wlat, wkr, ku, vu, wo, wg, wu, wd, cl, cr,
     xbuf, xf, qs, qrv, sqs, sqr, lats, latr, qe, qbuf, accs, accr, mls, mlr,
     nls, nks, osend, obuf, ohs, h3, tall, es, er, ab, sqas, sqa, psq, attf, mids,
-    gs, us, gr, ur, sqms, sqmr, hb, ls, lr,
+    gs, us, gr, ur, sqms, sqmr, hb, ls, lr, wide_ref, kus, vus,
     wsem, ssem, rsem,
 ):
     k = lax.axis_index("kv")
@@ -208,22 +208,22 @@
     D = W * K
     B = R * T
     LAT = h_wlat.shape[1]
-    ROPE = h_wkr.shape[1]
+    ROPE = h_wkr.shape[0]
     QN = h_wqn.shape[1]
     QR = h_wqr.shape[1]
     HD = QR // ROPE
     NOPE = QN // HD
     H = HD * T
-    VD = h_vu.shape[1] // HD
+    VD = h_vu.shape[1]
     half = ROPE // 2
     score_scale = (NOPE + ROPE) ** (-0.5)
     col = pl.ds(pl.multiple_of(k * W, 128), W)
 
     loads = {}
     pairs = [
-        ("qn", h_wqn, wqn), ("qr", h_wqr, wqr), ("lat", h_wlat, wlat),
-        ("kr", h_wkr.at[col], wkr), ("ku", h_ku, ku), ("cl", h_cl, cl), ("cr", h_cr, cr),
-        ("vu", h_vu, vu), ("wo", h_wo, wo), ("wg", h_wg, wg), ("wu", h_wu, wu), ("wd", h_wd, wd),
+        ("lat", h_wlat, wlat), ("kr", h_wkr.at[:, col], wkr), ("ku", h_ku, ku),
+        ("qn", h_wqn, wqn), ("qr", h_wqr, wqr), ("vu", h_vu, vu), ("cl", h_cl, cl), ("cr", h_cr, cr),
+        ("wo", h_wo, wo), ("wg", h_wg, wg), ("wu", h_wu, wu), ("wd", h_wd, wd),
     ]
     for i, (name, src, dst) in enumerate(pairs):
         loads[name] = pltpu.make_async_copy(src, dst, wsem.at[i])
@@ -275,22 +275,36 @@
     def all_rows(ref):
         return jnp.concatenate([ref[c] for c in range(ref.shape[0])], axis=1)
 
+    gain_start = pl.multiple_of(k * (W // 128), W // 128)
+
+    def gain_row(g):
+        g = g.astype(F32)
+        return jnp.concatenate([g[i:i + 1] for i in range(g.shape[0])], axis=1)
+
+    def by_head(src, dst):
+        n = src.shape[1]
+        wide_ref[...] = src[...].astype(F32)
+        for h in range(HD):
+            dst[:, h * n:(h + 1) * n] = wide_ref[pl.ds(h, LAT, stride=HD), :].astype(BF16)
+
     pl.semaphore_wait(barrier, len(others))
 
     copies = [send(resid, xbuf.at[t], off) for off in tps]
     xo = resid[...].astype(F32)
     xbuf[pl.ds(t, 1)] = resid[...][None]
-    again = attn_gain[:, col].astype(F32)
+    again = gain_row(attn_gain[pl.ds(gain_start, W // 128), :])
     own_normed = (xo * again).astype(BF16)
     loads["lat"].wait()
     loads["kr"].wait()
     lats[:, :LAT] = dot(own_normed, wlat)
-    lats[:, LAT:LAT + ROPE] = dot(own_normed, wkr)
+    lats[:, LAT:LAT + ROPE] = dot_nt(own_normed, wkr[...])
     lats[:, LAT + ROPE:] = jnp.broadcast_to(
         jnp.sum(xo * xo, axis=1, keepdims=True), (R, lats.shape[1] - LAT - ROPE)
     )
     latr[pl.ds(k, 1)] = lats[...][None]
     lat_copies = [send(lats, latr.at[k], off) for off in kvs]
+    loads["ku"].wait()
+    by_head(ku, kus)
     arrive(copies)
     for s in range(T):
         put_rows(xf, s, xbuf[s].astype(F32))
@@ -314,7 +328,7 @@
     raw = lat[:, :LAT]
     new_lat = (
         raw * lax.rsqrt(jnp.mean(raw * raw, axis=1, keepdims=True) + EPS)
-        * latent_gain[...].astype(F32)
+        * gain_row(latent_gain[...])
     ).astype(BF16)
     own_scale = lax.rsqrt(lat[:, LAT + ROPE:LAT + ROPE + 1] / D + EPS)
     tail = lat[:, LAT:]
@@ -349,10 +363,11 @@
     qe[:, :, LAT:] = jnp.dot(
         spread(q_rope, ROPE), fold, preferred_element_type=F32
     ).reshape(T, HD, RP).astype(BF16)
-    loads["ku"].wait()
-    qe[:, :, :LAT] = dot_nt(spread(q_nope, NOPE), ku[...]).reshape(T, HD, LAT).astype(BF16)
+    qe[:, :, :LAT] = dot_nt(spread(q_nope, NOPE), kus[...]).reshape(T, HD, LAT).astype(BF16)
     copies = [send(qe.at[peer(off)[1]], qbuf.at[k, t], off) for off in others]
     qbuf[pl.ds(k, 1), pl.ds(t, 1)] = qe[pl.ds(t, 1)][None]
+    loads["vu"].wait()
+    by_head(vu, vus)
     loads["cl"].wait()
     loads["cr"].wait()
     arrive(copies)
@@ -364,7 +379,9 @@
         qb = qb32.astype(BF16)
         keys = cl[pl.ds(b, 1)][0]
         scores = (
-            dot_nt(qb[:, :LAT], keys) + dot_nt(qb[:, LAT:LAT + ROPE], cr[pl.ds(b, 1)][0])
+            dot_nt(qb[:, :LAT], keys) + jnp.dot(
+                qb[:, LAT:LAT + ROPE], cr[pl.ds(b, 1)][0], preferred_element_type=F32
+            )
         ) * score_scale
         m = jnp.max(scores, axis=1, keepdims=True)
         p = jnp.exp(scores - m)
@@ -400,9 +417,8 @@
     osend[...] = (summed / total).reshape(T, HD, LAT).astype(BF16)
     copies = [send(osend.at[peer(off)[1]], obuf.at[t], off) for off in tps]
     obuf[pl.ds(t, 1)] = osend[pl.ds(t, 1)]
-    loads["vu"].wait()
-    arrive(copies)
-    wide = dot(obuf[...].astype(F32).reshape(T * HD, LAT).astype(BF16), vu)
+    arrive(copies)
+    wide = dot(obuf[...].astype(F32).reshape(T * HD, LAT).astype(BF16), vus)
     mask = own_head(HD * VD, VD)
     for i in range(T):
         ohs[i:i + 1, :] = jnp.sum(
@@ -430,20 +446,20 @@
         psq[pl.ds(s, R, stride=T), :] = sum(sqa[j, s] for j in range(K))
     post_scale = lax.rsqrt(psq[...][:, :1] / D + EPS)
     mid = (
-        x + all_rows(attf) * post_scale * post_gain[:, col].astype(F32)
+        x + all_rows(attf) * post_scale * gain_row(post_gain[pl.ds(gain_start, W // 128), :])
     ).astype(BF16).astype(F32)
     put_all(mids, mid)
-    normed_m = (mid * mlp_gain[:, col].astype(F32)).astype(BF16)
+    normed_m = (mid * gain_row(mlp_gain[pl.ds(gain_start, W // 128), :])).astype(BF16)
     sqms[...] = jnp.broadcast_to(
         jnp.sum(mid * mid, axis=1, keepdims=True), (B, 128)
     ).reshape(K, T, 128)
-    FD = wg.shape[1]
+    FD = wg.shape[0]
     loads["wg"].wait()
-    gs[...] = dot(normed_m, wg).reshape(K, T, FD).astype(BF16)
+    gs[...] = dot_nt(normed_m, wg[...]).reshape(K, T, FD).astype(BF16)
     copies = [send(gs.at[peer(off)[0]], gr.at[k], off) for off in kvs]
     copies += [send(sqms.at[peer(off)[0]], sqmr.at[k], off) for off in kvs]
     loads["wu"].wait()
-    us[...] = dot(normed_m, wu).reshape(K, T, FD).astype(BF16)
+    us[...] = dot_nt(normed_m, wu[...]).reshape(K, T, FD).astype(BF16)
     copies += [send(us.at[peer(off)[0]], ur.at[k], off) for off in kvs]
     gr[pl.ds(k, 1)] = gs[pl.ds(k, 1)]
     ur[pl.ds(k, 1)] = us[pl.ds(k, 1)]
@@ -477,8 +493,10 @@
     T = lax.axis_size("tp")
     R, W = resid.shape
     LAT, HD, _ = key_up.shape
-    key_flat = key_up.reshape(LAT, -1)
-    value_flat = value_up.reshape(LAT, -1)
+    key_flat = key_up.reshape(LAT * HD, -1)
+    value_flat = value_up.reshape(LAT * HD, -1)
+    key_turned, rope_turned = w_key_rope.T, jnp.swapaxes(cache_rope_key, 1, 2)
+    gate_turned, up_turned = w_gate.T, w_up.T
     ROPE = w_key_rope.shape[1]
     half = ROPE // 2
     context = cache_latent.shape[1] * K
@@ -487,12 +505,13 @@
     sin = np.tile(np.concatenate([-np.sin(angle), np.sin(angle)]), HD)[None].astype(np.float32)
     B = R * T
     H = HD * T
-    QN, QR, FD, HV = w_query_nope.shape[1], w_query_rope.shape[1], w_gate.shape[1], value_flat.shape[1]
-    big = (w_query_nope, w_query_rope, w_latent, w_key_rope, key_flat, value_flat, w_out, w_gate,
-           w_up, w_down, cache_latent, cache_rope_key)
+    QN, QR, FD = w_query_nope.shape[1], w_query_rope.shape[1], w_gate.shape[1]
+    HV = HD * value_up.shape[2]
+    big = (w_query_nope, w_query_rope, w_latent, key_turned, key_flat, value_flat, w_out,
+           gate_turned, up_turned, w_down, cache_latent, rope_turned)
 
     def held(a):
-        return pltpu.VMEM((W, ROPE) if a is w_key_rope else a.shape, a.dtype)
+        return pltpu.VMEM((ROPE, W) if a is key_turned else a.shape, a.dtype)
 
     def bf(*shape):
         return pltpu.VMEM(shape, BF16)
@@ -510,6 +529,7 @@
         fl(R, 128), fl(K, T, R, 128), fl(B, 128), slabs, slabs,
         bf(K, T, FD), bf(K, T, FD), bf(K, T, FD), bf(K, T, FD), fl(K, T, 128), fl(K, T, 128),
         bf(K, T, FD), bf(T, R, W), bf(T, R, W),
+        fl(*key_flat.shape), bf(LAT, QN), bf(LAT, HV),
     ]
     count = 10 * (K - 1) + 5 * (T - 1) + 2 * (K * T - 1) + 8
     vmem = pl.BlockSpec(memory_space=pltpu.VMEM)
@@ -532,7 +552,7 @@
             collective_id=0, has_side_effects=True, vmem_limit_bytes=60 * 1024 * 1024
         ),
     )(
-        resid, attn_gain[None], latent_gain[None], post_gain[None], mlp_gain[None],
+        resid, *(g.reshape(-1, 128) for g in (attn_gain, latent_gain, post_gain, mlp_gain)),
         jnp.asarray(cos), jnp.asarray(sin), *big,
     )
 

time: 91.2 us -> 70.9 us (0.78)
  local copies, waits for them, and re-layouts: 24.4 us -> 3.79 us
    unnamed x9 -> x3, local copies, waits for them, and re-layouts: 15.8 us -> 3.79 us
    broadcast_in_dim x4 -> x0, local copies, waits for them, and re-layouts: 5.18 us -> none  [the longest x1 1.31 us: fused(): attn_gain[None]]
    reshape x1 -> x0, local copies, waits for them, and re-layouts: 3.46 us -> none  [fused(): value_flat = value_up.reshape(LAT, -1)]
where the time goes in v2:
time: 70.9 us; the launch traced here: 70.6 us
  Pallas kernels  66.2 us (93%)
  local copies, waits for them, and re-layouts  3.79 us (5%)
    pallas_call x1, Pallas kernels, fused(): pl.pallas_call(functools.partial(layer_kernel, K, T, context), out_shape=...  66.2 us
    unnamed x3, local copies, waits for them, and re-layouts  3.79 us

profile of v2, /device:TPU:0, one launch (start us, length us, event | category | flops | bytes accessed | tf_op | source)
XLA Modules:
  0.0 70.6 jit_solution(912831229398468739)
XLA Ops:
  0.6 66.2 %shard_map.202 = (bf16[4,1024]{1,0:T(4,128)(2,1)}, bf16[4,512]{1,0:T(4,128)(2,1)}, bf16[4,64]{1,0:T(4,128)(2,1)}) custom-call(bf16[4,1024]{1,0:T(4,128)(2,1)} %resid.1, bf16[32,128]{1,0:T(8,128)(2,1)} %bitcast.16, bf16[4,128]{1,0:T(4,128)(2,1)} %bitcast.19, bf16[32,128]{1,0:T(8,128)(2,1)} %bitcast.17, bf16[32,128]{1,0:T(8,128)(2,1)} %bitcast.18, ...), custom_call_target="tpu_custom_call" | custom-call | tf_op jit(solution)/shard_map/pallas_call | solution.py:537
  66.8 1.3 %copy.25 = bf16[4,1024]{1,0:T(4,128)(2,1)} copy(bf16[4,1024]{1,0:T(4,128)(2,1)} %get-tuple-element.6) | data formatting | bytes 16384
  68.1 1.3 %copy.26 = bf16[4,512]{1,0:T(4,128)(2,1)} copy(bf16[4,512]{1,0:T(4,128)(2,1)} %get-tuple-element.7) | data formatting | bytes 8192
  69.4 1.2 %copy.27 = bf16[4,64]{1,0:T(4,128)(2,1)} copy(bf16[4,64]{1,0:T(4,128)(2,1)} %get-tuple-element.8) | data formatting | bytes 1024

commit v3 on v2

--- a/solution.py
+++ b/solution.py
@@ -287,9 +287,6 @@
         for h in range(HD):
             dst[:, h * n:(h + 1) * n] = wide_ref[pl.ds(h, LAT, stride=HD), :].astype(BF16)
 
-    pl.semaphore_wait(barrier, len(others))
-
-    copies = [send(resid, xbuf.at[t], off) for off in tps]
     xo = resid[...].astype(F32)
     xbuf[pl.ds(t, 1)] = resid[...][None]
     again = gain_row(attn_gain[pl.ds(gain_start, W // 128), :])
@@ -302,6 +299,8 @@
         jnp.sum(xo * xo, axis=1, keepdims=True), (R, lats.shape[1] - LAT - ROPE)
     )
     latr[pl.ds(k, 1)] = lats[...][None]
+    pl.semaphore_wait(barrier, len(others))
+    copies = [send(resid, xbuf.at[t], off) for off in tps]
     lat_copies = [send(lats, latr.at[k], off) for off in kvs]
     loads["ku"].wait()
     by_head(ku, kus)
@@ -323,6 +322,8 @@
     qrv[pl.ds(k, 1)] = qs[pl.ds(k, 1)]
     sqr[pl.ds(k, 1)] = sqs[pl.ds(k, 1)]
 
+    loads["vu"].wait()
+    by_head(vu, vus)
     arrive(lat_copies)
     lat = sum(latr[s] for s in range(K))
     raw = lat[:, :LAT]
@@ -364,17 +365,23 @@
         spread(q_rope, ROPE), fold, preferred_element_type=F32
     ).reshape(T, HD, RP).astype(BF16)
     qe[:, :, :LAT] = dot_nt(spread(q_nope, NOPE), kus[...]).reshape(T, HD, LAT).astype(BF16)
-    copies = [send(qe.at[peer(off)[1]], qbuf.at[k, t], off) for off in others]
+    copies = [send(qe.at[peer(off)[1]], qbuf.at[k, t], off) for off in tps]
+    relayed = {off: [send(qe.at[t], qbuf.at[k, t], off)] for off in kvs}
     qbuf[pl.ds(k, 1), pl.ds(t, 1)] = qe[pl.ds(t, 1)][None]
-    loads["vu"].wait()
-    by_head(vu, vus)
+    for away, copy in zip(tps, copies):
+        copy.wait_recv()
+        slot = qbuf.at[k, lax.rem(t + T - away[1], T)]
+        for off in kvs:
+            relayed[off].append(send(slot, slot, off))
     loads["cl"].wait()
     loads["cr"].wait()
-    arrive(copies)
 
     copies = []
-    for off in kvs + [(0, 0)]:
+    own_qb = None
+    for off in [(0, 0)] + kvs:
         b = peer(off)[0]
+        if off != (0, 0):
+            arrive(relayed[(K - off[0], 0)])
         qb32 = qbuf[pl.ds(b, 1)][0].astype(F32).reshape(H, LAT + RP)
         qb = qb32.astype(BF16)
         keys = cl[pl.ds(b, 1)][0]
@@ -389,6 +396,7 @@
         acc = jnp.dot(p.astype(BF16), keys, preferred_element_type=F32).astype(BF16)
         ml = jnp.where(lane_iota((H, 128)) < 64, m, total)
         if off == (0, 0):
+            own_qb = qb32
             accr[pl.ds(k, 1)] = acc[None]
             mlr[pl.ds(k, 1)] = ml[None]
         else:
@@ -399,8 +407,8 @@
     nl = nls[pl.ds(k, 1), :]
     nk = nks[pl.ds(k, 1), :]
     own_score = (
-        jnp.sum(qb32[:, :LAT] * nl, axis=1, keepdims=True)
-        + jnp.sum(qb32[:, LAT:] * nk, axis=1, keepdims=True)
+        jnp.sum(own_qb[:, :LAT] * nl, axis=1, keepdims=True)
+        + jnp.sum(own_qb[:, LAT:] * nk, axis=1, keepdims=True)
     ) * score_scale
     arrive(copies)
     peaks = [mlr[s][:, :1] for s in range(K)]
@@ -483,6 +491,11 @@
     out[...] = (mid_own + lowered).astype(BF16)
     for copy in sent:
         copy.wait_send()
+
+
+def hand_over(a, b, c, a_out, b_out, c_out):
+    for src, dst in ((a, a_out), (b, b_out), (c, c_out)):
+        dst[...] = src[...]
 
 
 def fused(
@@ -534,13 +547,14 @@
     count = 10 * (K - 1) + 5 * (T - 1) + 2 * (K * T - 1) + 8
     vmem = pl.BlockSpec(memory_space=pltpu.VMEM)
     hbm = pl.BlockSpec(memory_space=pl.ANY)
-    return pl.pallas_call(
+    out_shape = (
+        jax.ShapeDtypeStruct((R, W), BF16),
+        jax.ShapeDtypeStruct((R, LAT), BF16),
+        jax.ShapeDtypeStruct((R, ROPE), BF16),
+    )
+    made = pl.pallas_call(
         functools.partial(layer_kernel, K, T, context),
-        out_shape=(
-            jax.ShapeDtypeStruct((R, W), BF16),
-            jax.ShapeDtypeStruct((R, LAT), BF16),
-            jax.ShapeDtypeStruct((R, ROPE), BF16),
-        ),
+        out_shape=out_shape,
         in_specs=[vmem] * 7 + [hbm] * len(big),
         out_specs=(vmem, vmem, vmem),
         scratch_shapes=scratch + [
@@ -555,6 +569,9 @@
         resid, *(g.reshape(-1, 128) for g in (attn_gain, latent_gain, post_gain, mlp_gain)),
         jnp.asarray(cos), jnp.asarray(sin), *big,
     )
+    return pl.pallas_call(
+        hand_over, out_shape=out_shape, in_specs=[vmem] * 3, out_specs=(vmem,) * 3
+    )(*made)
 
 
 def layer(*args):

time: 70.9 us -> 67.2 us (0.948)
  local copies, waits for them, and re-layouts: 3.79 us -> 0 us
    unnamed x3 -> x0, local copies, waits for them, and re-layouts: 3.79 us -> none
    pallas_call x0 -> x1, Pallas kernels: none -> 1.31 us  [fused(): pl.pallas_call(hand_over, out_shape=out_shape, in_specs=[vmem] * 3, out_s...]
    pallas_call x1, Pallas kernels: 66.2 us -> 65 us  [fused(): pl.pallas_call(functools.partial(layer_kernel, K, T, context), out_shape=...]
where the time goes in v3:
time: 67.2 us; the launch traced here: 67 us
  Pallas kernels  66.3 us (99%)
    pallas_call x1, Pallas kernels, fused(): pl.pallas_call(functools.partial(layer_kernel, K, T, context), out_shape=...  65 us

profile of v3, /device:TPU:0, one launch (start us, length us, event | category | flops | bytes accessed | tf_op | source)
XLA Modules:
  0.0 67.0 jit_solution(835924858568749507)
XLA Ops:
  0.6 65.0 %shard_map.202 = (bf16[4,1024]{1,0:T(4,128)(2,1)}, bf16[4,512]{1,0:T(4,128)(2,1)}, bf16[4,64]{1,0:T(4,128)(2,1)}) custom-call(bf16[4,1024]{1,0:T(4,128)(2,1)} %resid.1, bf16[32,128]{1,0:T(8,128)(2,1)} %bitcast.16, bf16[4,128]{1,0:T(4,128)(2,1)} %bitcast.19, bf16[32,128]{1,0:T(8,128)(2,1)} %bitcast.17, bf16[32,128]{1,0:T(8,128)(2,1)} %bitcast.18, ...), custom_call_target="tpu_custom_call" | custom-call | tf_op jit(solution)/shard_map/pallas_call | solution.py:555
  65.7 1.3 %shard_map.203 = (bf16[4,1024]{1,0:T(4,128)(2,1)}, bf16[4,512]{1,0:T(4,128)(2,1)}, bf16[4,64]{1,0:T(4,128)(2,1)}) custom-call(bf16[4,1024]{1,0:T(4,128)(2,1)} %get-tuple-element.6.a, bf16[4,512]{1,0:T(4,128)(2,1)} %get-tuple-element.7.b, bf16[4,64]{1,0:T(4,128)(2,1)} %get-tuple-element.8.c), custom_call_target="tpu_custom_call" | custom-call | tf_op jit(solution)/shard_map/pallas_call | solution.py:572
